TPU v7x, 32 devices: a whole 2x2x4 slice. The times are simulated.
32 devices in a mesh: sp: 4 (over z), fs: 4 (over y, x), tp: 2 (over core).
Axes of the slice: x: 2, y: 2, z: 4, core: 2. Of those that a mesh axis runs over, the one named last changes fastest.
Arguments:
- tokens: bfloat16 [4, 640, 2048], P('fs', 'sp', 'tp'), may hold values from -6 to 6
- mix_gain: float32 [2048], replicated, may hold values from 0.1 to 1.9
- conv_b_weight: bfloat16 [2048, 1024], P(('sp', 'fs'), 'tp'), may hold values from -0.125 to 0.125
- conv_c_weight: bfloat16 [2048, 1024], P(('sp', 'fs'), 'tp'), may hold values from -0.125 to 0.125
- conv_v_weight: bfloat16 [2048, 1024], P(('sp', 'fs'), 'tp'), may hold values from -0.125 to 0.125
- conv_taps: float32 [3, 1024], P(None, 'tp'), may hold values from -3.5 to 3.5
- query_weight: bfloat16 [2048, 2048], P(('sp', 'fs'), 'tp'), may hold values from -0.125 to 0.125
- query_rope_weight: bfloat16 [2048, 1024], P(('sp', 'fs'), 'tp'), may hold values from -4.5 to 4.5
- latent_weight: bfloat16 [2048, 512], P(('sp', 'fs')), may hold values from -0.125 to 0.125
- key_rope_weight: bfloat16 [2048, 64], replicated, may hold values from -1 to 1
- latent_gain: float32 [512], replicated, may hold values from 0.1 to 1.9
- key_up_weight: bfloat16 [512, 2048], P(None, 'tp'), may hold values from -0.25 to 0.25
- value_up_weight: bfloat16 [512, 2048], P(None, 'tp'), may hold values from -0.25 to 0.25
- head_gain: float32 [2048], P('tp'), may hold values from 0.1 to 1.9
- conv_out_weight: bfloat16 [1024, 2048], P('tp', ('sp', 'fs')), may hold values from -0.109375 to 0.109375
- attn_out_weight: bfloat16 [2048, 2048], P('tp', ('sp', 'fs')), may hold values from -0.109375 to 0.109375
Outputs:
- mixed: bfloat16 [4, 640, 2048], P('fs', ('sp', 'tp'))
All inputs are finite; a program needn't handle non-finite values.
Results may differ from a plain program's by a relative error of at most 0.025.
Values may be sent and summed in bfloat16 or wider, within the bound.
No kernel may reach another device: no remote copies, remote signals or barrier semaphores. Data moves between devices by JAX's collectives and lax.ppermute only.
A program may use at most 128 MiB of HBM per device.

v0:
```python
import jax
import jax.numpy as jnp
from jax import lax
from jax.sharding import PartitionSpec as P

NOPE = 128
ROPE = 64
VD = 128
KVL = 512
SEG = 64
norm_epsilon = 1e-06
rope_theta = 10000.0


def passed_along(block, axis, distance):
    devices = range(lax.axis_size(axis))
    route = [(i - distance, i) for i in devices if i - distance in devices]
    return lax.ppermute(block, axis, route)


def rms_scale(values, gain):
    return (
        values * lax.rsqrt(jnp.mean(values * values, axis=-1, keepdims=True) + norm_epsilon) * gain
    )


def rope_tables(positions):
    half_width = ROPE // 2
    frequency = rope_theta ** (-jnp.arange(half_width, dtype=jnp.float32) * 2.0 / ROPE)
    angles = positions[:, None] * frequency[None, :]
    return (jnp.cos(angles), jnp.sin(angles))


def rotate(values, cosine, sine):
    half_width = ROPE // 2
    first = values[..., :half_width]
    second = values[..., half_width:]
    return jnp.concatenate(
        [first * cosine - second * sine, second * cosine + first * sine], axis=-1
    )


def shards(
    tokens,
    mix_gain,
    conv_b_weight,
    conv_c_weight,
    conv_v_weight,
    conv_taps,
    query_weight,
    query_rope_weight,
    latent_weight,
    key_rope_weight,
    latent_gain,
    key_up_weight,
    value_up_weight,
    head_gain,
    conv_out_weight,
    attn_out_weight,
):
    full_rows = lax.all_gather(tokens[0], "tp", axis=1, tiled=True)
    tok_rows = full_rows.shape[0]
    normed = rms_scale(full_rows.astype(jnp.float32), mix_gain).astype(jnp.bfloat16)
    offset = lax.axis_index("sp") * tok_rows
    token_index = offset + jnp.arange(tok_rows, dtype=jnp.int32)
    cosine, sine = rope_tables(token_index.astype(jnp.float32))
    local_heads = query_weight.shape[1] // NOPE
    count_sp = lax.axis_size("sp")
    count_fs = lax.axis_size("fs")
    count_tp = lax.axis_size("tp")
    fs_index = lax.axis_index("fs")
    row_piece = normed.shape[1] // (count_sp * count_fs)
    all_normed = lax.all_gather(normed, "fs", axis=0, tiled=True)
    picked = lax.dynamic_index_in_dim(
        all_normed.reshape(-1, count_sp, count_fs, row_piece), fs_index, 2, keepdims=False
    ).reshape(-1, count_sp * row_piece)
    gathered = (
        lax.all_gather(conv_b_weight, "sp", axis=0, tiled=True),
        lax.all_gather(conv_c_weight, "sp", axis=0, tiled=True),
        lax.all_gather(conv_v_weight, "sp", axis=0, tiled=True),
        lax.all_gather(query_weight, "sp", axis=0, tiled=True),
        lax.all_gather(query_rope_weight, "sp", axis=0, tiled=True),
        lax.all_gather(latent_weight, "sp", axis=0, tiled=True),
    )

    def project_in():
        return jnp.concatenate(
            [jnp.dot(picked, member, preferred_element_type=jnp.float32) for member in gathered],
            axis=1,
        )

    joined = lax.psum_scatter(
        project_in().astype(jnp.bfloat16), "fs", scatter_dimension=0, tiled=True
    ).astype(jnp.float32)
    bounds = []
    running_total = 0
    for member in gathered[:-1]:
        running_total = running_total + member.shape[1]
        bounds.append(running_total)
    sums = tuple(jnp.split(joined, bounds, axis=1))
    latent_raw = sums[5].astype(jnp.bfloat16)
    gate_b = sums[0].astype(jnp.bfloat16)
    gate_c = sums[1].astype(jnp.bfloat16)
    values_v = sums[2].astype(jnp.bfloat16)
    query_nope = sums[3].astype(jnp.bfloat16).reshape(tok_rows, local_heads, NOPE)
    query_rot = rotate(
        sums[4].reshape(tok_rows, local_heads, ROPE), cosine[:, None, :], sine[:, None, :]
    ).astype(jnp.bfloat16)
    latent = rms_scale(latent_raw.astype(jnp.float32), latent_gain).astype(jnp.bfloat16)
    key_rot = rotate(
        jnp.dot(normed, key_rope_weight, preferred_element_type=jnp.float32), cosine, sine
    ).astype(jnp.bfloat16)
    query_latent = jnp.einsum(
        "thn,khn->thk",
        query_nope,
        key_up_weight.reshape(KVL, local_heads, NOPE),
        preferred_element_type=jnp.float32,
    ).astype(jnp.bfloat16)
    attn_scale = (NOPE + ROPE) ** (-0.5)
    product = (gate_c.astype(jnp.float32) * values_v.astype(jnp.float32)).astype(jnp.bfloat16)
    previous = passed_along(product[tok_rows - 2 :], "sp", 1)
    padded = jnp.concatenate([previous, product], axis=0).astype(jnp.float32)
    convolved = (
        conv_taps[0] * padded[0:tok_rows]
        + conv_taps[1] * padded[1 : tok_rows + 1]
        + conv_taps[2] * padded[2 : tok_rows + 2]
    )
    conv_y = (gate_b.astype(jnp.float32) * convolved).astype(jnp.bfloat16)
    query_segment = token_index // SEG
    last_segment = (offset + tok_rows - 1) // SEG

    def key_block(running, latent_block, rot_block, first_key):
        peak_old, denom_old, accum_old = running
        block_rows = latent_block.shape[0]
        scores = (
            jnp.einsum(
                "thk,jk->thj", query_latent, latent_block, preferred_element_type=jnp.float32
            )
            + jnp.einsum("thr,jr->thj", query_rot, rot_block, preferred_element_type=jnp.float32)
        ) * attn_scale
        key_segment = (first_key + jnp.arange(block_rows, dtype=jnp.int32)) // SEG
        allowed = key_segment[None, None, :] <= query_segment[:, None, None]
        peak_new = jnp.maximum(peak_old, jnp.max(jnp.where(allowed, scores, -1e30), axis=-1))
        weights = jnp.where(allowed, jnp.exp(scores - peak_new[..., None]), 0.0)
        rescale = jnp.exp(peak_old - peak_new)
        denom_new = denom_old * rescale + jnp.sum(weights, axis=-1)
        accum_new = accum_old * rescale[..., None] + jnp.einsum(
            "thj,jk->thk",
            weights.astype(jnp.bfloat16),
            latent_block,
            preferred_element_type=jnp.float32,
        )
        return (peak_new, denom_new, accum_new)

    starting = (
        jnp.full((tok_rows, local_heads), -1e30, jnp.float32),
        jnp.zeros((tok_rows, local_heads), jnp.float32),
        jnp.zeros((tok_rows, local_heads, KVL), jnp.float32),
    )
    latent_piece = lax.all_gather(latent, "sp", axis=0, tiled=True)
    rot_piece = lax.all_gather(key_rot, "sp", axis=0, tiled=True)
    piece_rows = latent_piece.shape[0]
    splits = max(1, piece_rows // 512)
    while piece_rows % splits:
        splits = splits - 1
    block_rows = piece_rows // splits

    def visit(state, block_index):
        block_begin = block_index * block_rows
        latent_block = lax.dynamic_slice_in_dim(latent_piece, block_begin, block_rows, 0)
        rot_block = lax.dynamic_slice_in_dim(rot_piece, block_begin, block_rows, 0)
        updated = lax.cond(
            block_begin // SEG <= last_segment,
            lambda inner: key_block(inner, latent_block, rot_block, block_begin),
            lambda inner: inner,
            state,
        )
        return (updated, None)

    peak, denom, accum = lax.scan(visit, starting, jnp.arange(splits, dtype=jnp.int32))[0]
    attended = (accum / denom[..., None]).astype(jnp.bfloat16)
    head_out = jnp.einsum(
        "thk,khv->thv",
        attended,
        value_up_weight.reshape(KVL, local_heads, VD),
        preferred_element_type=jnp.float32,
    )
    normed_heads = rms_scale(head_out, head_gain.reshape(local_heads, VD))
    attn_y = normed_heads.astype(jnp.bfloat16).reshape(tok_rows, local_heads * VD)
    share_rows = tok_rows // count_tp
    conv_all, attn_all = (
        lax.all_gather(conv_y, "fs", axis=0, tiled=True),
        lax.all_gather(attn_y, "fs", axis=0, tiled=True),
    )
    conv_sorted = (
        conv_all.reshape(count_fs, count_tp, share_rows, -1)
        .transpose(1, 0, 2, 3)
        .reshape(count_fs * tok_rows, -1)
    )
    attn_sorted = (
        attn_all.reshape(count_fs, count_tp, share_rows, -1)
        .transpose(1, 0, 2, 3)
        .reshape(count_fs * tok_rows, -1)
    )
    conv_cols_sp, attn_cols_sp = (
        lax.all_gather(conv_out_weight, "sp", axis=1, tiled=True),
        lax.all_gather(attn_out_weight, "sp", axis=1, tiled=True),
    )
    col_sums = lax.psum_scatter(
        (
            jnp.dot(conv_sorted, conv_cols_sp, preferred_element_type=jnp.float32)
            + jnp.dot(attn_sorted, attn_cols_sp, preferred_element_type=jnp.float32)
        ).astype(jnp.bfloat16),
        "tp",
        scatter_dimension=0,
        tiled=True,
    )
    col_piece = conv_cols_sp.shape[1] // count_sp
    outgoing = col_sums.reshape(count_fs, share_rows, count_sp * col_piece)
    arrived = lax.all_to_all(outgoing, "fs", split_axis=0, concat_axis=2, tiled=True)
    result = (
        arrived.reshape(share_rows, count_fs, count_sp, col_piece)
        .transpose(0, 2, 1, 3)
        .reshape(share_rows, count_fs * count_sp * col_piece)
    )
    return result[None]


def solution(mesh):
    return jax.shard_map(
        shards,
        mesh=mesh,
        in_specs=(
            P("fs", "sp", "tp"),
            P(),
            P(("sp", "fs"), "tp"),
            P(("sp", "fs"), "tp"),
            P(("sp", "fs"), "tp"),
            P(None, "tp"),
            P(("sp", "fs"), "tp"),
            P(("sp", "fs"), "tp"),
            P(("sp", "fs"), None),
            P(),
            P(),
            P(None, "tp"),
            P(None, "tp"),
            P("tp"),
            P("tp", ("sp", "fs")),
            P("tp", ("sp", "fs")),
        ),
        out_specs=P("fs", ("sp", "tp"), None),
        check_vma=False,
    )
```

profile of v0, /device:TPU:0, one launch (start us, length us, event | category | flops | bytes accessed | tf_op | source)
XLA Modules:
  0.0 311.9 jit_solution(16413146177102707444)
XLA Ops:
  6.6 2.7 all-gather
  9.5 1.8 fusion.22
  12.2 17.5 %all_gather.44 = bf16[512,512]{1,0:T(8,128)(2,1)S(1)} all-gather(bf16[128,512]{1,0:T(8,128)(2,1)S(1)} %copy-done.9), channel_id=1, replica_groups=mesh['sp'=4,'fs'=4,'tp'=2] {'sp'}, dimensions={0}, use_global_device_ids=true | all-gather | bytes 655360 | tf_op jit(solution)/shard_map/all_gather | solution.py:78
  29.6 16.5 %all_gather.45 = bf16[512,512]{1,0:T(8,128)(2,1)} all-gather(bf16[128,512]{1,0:T(8,128)(2,1)S(1)} %copy-done.10), channel_id=1, replica_groups=mesh['sp'=4,'fs'=4,'tp'=2] {'sp'}, dimensions={0}, use_global_device_ids=true | all-gather | bytes 655360 | tf_op jit(solution)/shard_map/all_gather | solution.py:79
  46.1 16.7 %all_gather.46 = bf16[512,512]{1,0:T(8,128)(2,1)} all-gather(bf16[128,512]{1,0:T(8,128)(2,1)S(1)} %copy-done.11), channel_id=1, replica_groups=mesh['sp'=4,'fs'=4,'tp'=2] {'sp'}, dimensions={0}, use_global_device_ids=true | all-gather | bytes 655360 | tf_op jit(solution)/shard_map/all_gather | solution.py:80
  62.8 22.8 %all_gather.48 = bf16[512,512]{1,0:T(8,128)(2,1)S(1)} all-gather(bf16[128,512]{1,0:T(8,128)(2,1)S(1)} %copy-done.12), channel_id=1, replica_groups=mesh['sp'=4,'fs'=4,'tp'=2] {'sp'}, dimensions={0}, use_global_device_ids=true | all-gather | bytes 655360 | tf_op jit(solution)/shard_map/all_gather | solution.py:82
  85.6 17.8 %all_gather.49 = bf16[512,512]{1,0:T(8,128)(2,1)} all-gather(bf16[128,512]{1,0:T(8,128)(2,1)S(1)} %copy-done.13), channel_id=1, replica_groups=mesh['sp'=4,'fs'=4,'tp'=2] {'sp'}, dimensions={0}, use_global_device_ids=true | all-gather | bytes 655360 | tf_op jit(solution)/shard_map/all_gather | solution.py:83
  103.4 4.4 %copy.65 = bf16[640,2048]{0,1:T(8,128)(2,1)} copy(bf16[640,2048]{1,0:T(8,128)(2,1)} %all-gather.7.cloned.1.call-done) | data formatting | bytes 5242880 | tf_op jit(solution)/shard_map/all_gather | solution.py:73
  107.8 1.1 constant_dynamic-slice_fusion
  109.9 2.5 convolution_convert_fusion.5
  112.4 1.3 copy.69
  113.8 2.5 convolution_convert_fusion.4
  116.3 1.3 copy.70
  117.6 0.9 constant_dynamic-update-slice_fusion.2
  119.4 0.9 constant_dynamic-update-slice_fusion
  120.4 3.3 %fusion.15 = bf16[640,3584]{1,0:T(8,128)(2,1)} fusion(bf16[640,3584]{1,0:T(8,128)(2,1)} %constant_dynamic-update-slice_fusion, bf16[640,512]{0,1:T(8,128)(2,1)S(1)} %bitcast.104, bf16[512,1024]{1,0:T(8,128)(2,1)} %all-gather.9.cloned.1.call-done), kind=kOutput, calls=%fused_computation.35 | convolution fusion | flops 671744000 | bytes 3014656 | tf_op jit(solution)/shard_map/dot_general | solution.py:88
  123.6 1.4 fusion.19
  125.0 1.4 fusion.18
  126.6 1.0 copy-done.3
  128.4 1.9 broadcast_in_dim.56
  130.3 14.1 %all-gather.1 = bf16[4,160,64]{1,2,0:T(8,128)(2,1)} all-gather(bf16[1,160,64]{1,2,0:T(8,128)(2,1)S(1)} %maximum_bitcast_fusion), channel_id=1, replica_groups=mesh['sp'=4,'fs'=4,'tp'=2] {'sp'}, dimensions={0}, use_global_device_ids=true | all-gather | bytes 102400 | tf_op jit(solution)/shard_map/all_gather | solution.py:161
  144.3 36.4 %reduce-scatter.3.cloned.1.call-done = bf16[160,3584]{1,0:T(8,128)(2,1)} async-done(((bf16[640,3584]{1,0:T(8,128)(2,1)}), bf16[160,3584]{1,0:T(8,128)(2,1)}) %reduce-scatter.3.cloned.1.call-update) | async-done | bytes 1146896 | tf_op jit(solution)/shard_map/reduce_scatter | solution.py:92
  180.7 1.0 fusion.32
  181.8 1.8 fusion.34
  183.6 17.8 %all_gather.52 = bf16[640,512]{1,0:T(8,128)(2,1)S(1)} all-gather(bf16[160,512]{1,0:T(8,128)(2,1)S(1)} %get-tuple-element.251), channel_id=1, replica_groups=mesh['sp'=4,'fs'=4,'tp'=2] {'sp'}, dimensions={0}, use_global_device_ids=true | all-gather | bytes 819200 | tf_op jit(solution)/shard_map/all_gather | solution.py:160
  201.4 0.9 slice_convert_fusion
  203.0 1.5 fusion.16
  204.5 12.2 %conditional.1 = ((f32[160,8]{1,0:T(8,128)S(1)}, f32[160,8,512]{2,1,0:T(8,128)})) conditional(s32[]{:T(128)} %convert_element_type.79, (f32[160,8]{1,0:T(8,128)S(1)}, f32[160,8,512]{2,1,0:T(8,128)}) %tuple.31, (s32[160]{0:T(256)S(1)}, s32[160]{0:T(256)S(1)}, s32[]{:T(128)}, bf16[160,8,512]{2,0,1:T(8,128)(2,1)S(1)}, ...), branch_computations={%region_3.4_spmd, %region_4.7_spmd.clone} | conditional | flops 1792195712 | bytes 46272084 | solution.py:172
  204.9 1.7 copy.85
  206.5 1.7 reshape.204
  208.2 1.5 fusion.9
  209.7 1.9 select_reduce_fusion
  211.6 1.1 fusion.1
  213.3 1.8 multiply_add_fusion
  215.1 1.5 copy-done.2
  216.7 2.1 divide_convert_fusion
  218.8 1.1 multiply_reduce_fusion
  219.9 1.0 copy_bitcast_fusion
  221.6 2.5 collective-permute-start
  224.1 15.4 %all_gather.51 = bf16[512,512]{1,0:T(8,128)(2,1)S(1)} all-gather(bf16[512,128]{1,0:T(8,128)(2,1)S(1)} %copy-done.14), channel_id=1, replica_groups=mesh['sp'=4,'fs'=4,'tp'=2] {'sp'}, dimensions={1}, use_global_device_ids=true | all-gather | bytes 655360 | tf_op jit(solution)/shard_map/all_gather | solution.py:206
  239.5 1.0 fusion.40
  240.6 12.5 %all_gather.50 = bf16[640,512]{1,0:T(8,128)(2,1)S(1)} all-gather(bf16[160,512]{1,0:T(8,128)(2,1)S(1)} %fusion.40), channel_id=1, replica_groups=mesh['sp'=4,'fs'=4,'tp'=2] {'fs'}, dimensions={0}, use_global_device_ids=true | all-gather | bytes 819200 | tf_op jit(solution)/shard_map/all_gather | solution.py:192
  253.6 2.5 copy.81
  256.1 26.6 %all-gather.13.cloned.1.call-done = bf16[1024,512]{1,0:T(8,128)(2,1)} async-done(((bf16[1024,128]{1,0:T(8,128)(2,1)}), bf16[1024,512]{1,0:T(8,128)(2,1)}) %all-gather.13.cloned.1.call-update) | async-done | bytes 1048592 | tf_op jit(solution)/shard_map/all_gather | solution.py:207
  282.8 3.3 %fusion.17 = bf16[640,512]{1,0:T(8,128)(2,1)} fusion(f32[640,512]{1,0:T(8,128)S(1)} %fusion.44, bf16[640,1024]{1,0:T(8,128)(2,1)} %bitcast.98, bf16[1024,512]{1,0:T(8,128)(2,1)} %all-gather.13.cloned.1.call-done), kind=kOutput, calls=%fused_computation.38 | convolution fusion | flops 671744000 | bytes 4325376 | tf_op jit(solution)/shard_map/dot_general | solution.py:212
  286.1 6.5 %reduce-scatter.5.cloned.1.call-done = bf16[320,512]{1,0:T(8,128)(2,1)} async-done(((bf16[640,512]{1,0:T(8,128)(2,1)}), bf16[320,512]{1,0:T(8,128)(2,1)}) %reduce-scatter.5.cloned.1.call-update) | async-done | bytes 327696 | tf_op jit(solution)/shard_map/reduce_scatter | solution.py:209
  292.6 11.0 %all_to_all.15 = bf16[4,80,512]{2,1,0:T(8,128)(2,1)S(1)} all-to-all(bf16[4,80,512]{2,1,0:T(8,128)(2,1)} %bitcast.107), channel_id=1, replica_groups=mesh['sp'=4,'fs'=4,'tp'=2] {'fs'}, dimensions={0} | all-to-all | bytes 655360 | tf_op jit(solution)/shard_map/all_to_all | solution.py:220
  304.1 1.0 broadcast_in_dim_reshape.4
  (83 shorter events, 7.0 us)
Async XLA Ops:
  6.5 196.5 %copy-start = (bf16[512,1024]{1,0:T(8,128)(2,1)S(1)}, bf16[512,1024]{1,0:T(8,128)(2,1)}, u32[]{:S(2)}) copy-start(bf16[512,1024]{1,0:T(8,128)(2,1)} %param.29) | copy-start | bytes 3145732
  6.5 5.6 %copy-start.9 = (bf16[128,512]{1,0:T(8,128)(2,1)S(1)}, bf16[128,512]{1,0:T(8,128)(2,1)}, u32[]{:S(2)}) copy-start(bf16[128,512]{1,0:T(8,128)(2,1)} %param.20) | copy-start | bytes 393220
  6.5 23.1 %copy-start.10 = (bf16[128,512]{1,0:T(8,128)(2,1)S(1)}, bf16[128,512]{1,0:T(8,128)(2,1)}, u32[]{:S(2)}) copy-start(bf16[128,512]{1,0:T(8,128)(2,1)} %param.21) | copy-start | bytes 393220
  6.5 39.6 %copy-start.11 = (bf16[128,512]{1,0:T(8,128)(2,1)S(1)}, bf16[128,512]{1,0:T(8,128)(2,1)}, u32[]{:S(2)}) copy-start(bf16[128,512]{1,0:T(8,128)(2,1)} %param.22) | copy-start | bytes 393220
  6.5 96.9 %all-gather.7.cloned.1.call-start = ((), (), s32[]{:S(2)}) async-start(), calls=%async_computation.3 | async-start | bytes 3276800 | tf_op jit(solution)/shard_map/all_gather | solution.py:73
  9.3 53.5 %copy-start.12 = (bf16[128,512]{1,0:T(8,128)(2,1)S(1)}, bf16[128,512]{1,0:T(8,128)(2,1)}, u32[]{:S(2)}) copy-start(bf16[128,512]{1,0:T(8,128)(2,1)} %param.25) | copy-start | bytes 393220
  9.3 76.3 %copy-start.13 = (bf16[128,512]{1,0:T(8,128)(2,1)S(1)}, bf16[128,512]{1,0:T(8,128)(2,1)}, u32[]{:S(2)}) copy-start(bf16[128,512]{1,0:T(8,128)(2,1)} %param.26) | copy-start | bytes 393220
  11.4 109.0 %all-gather.9.cloned.1.call-start = ((), (), s32[]{:S(2)}) async-start(), calls=%async_computation.4 | async-start | bytes 1310720 | tf_op jit(solution)/shard_map/all_gather | solution.py:81
  12.1 168.6 %reduce-scatter.3.cloned.1.call-start = ((), (), s32[]{:S(2)}) async-start(), calls=%async_computation.5 | async-start | bytes 5734400 | tf_op jit(solution)/shard_map/reduce_scatter | solution.py:92
  109.0 4.8 %copy-start.5 = (bf16[640,4,1,128]{0,3,2,1:T(8,128)(2,1)}, bf16[640,4,1,128]{0,3,2,1:T(8,128)(2,1)S(1)}, u32[]{:S(2)}) copy-start(bf16[640,4,1,128]{0,3,2,1:T(8,128)(2,1)S(1)} %constant_dynamic-slice_fusion) | copy-start | bytes 1966084
  118.5 1.8 copy-start.6
  120.4 4.7 %copy-start.7 = (bf16[512,512]{1,0:T(8,128)(2,1)S(1)}, bf16[512,512]{1,0:T(8,128)(2,1)}, u32[]{:S(2)}) copy-start(bf16[512,512]{1,0:T(8,128)(2,1)} %all_gather.49) | copy-start | bytes 1572868
  126.5 1.1 copy-start.3
  126.5 1.1 copy-start.8
  126.5 55.3 %copy-start.17 = (f32[512]{0:T(512)S(1)}, f32[512]{0:T(512)}, u32[]{:S(2)}) copy-start(f32[512]{0:T(512)} %param.28) | copy-start | bytes 6148
  126.5 127.1 %all-gather.11.cloned.1.call-start = ((), (), s32[]{:S(2)}) async-start(), calls=%async_computation.6 | async-start | bytes 1638400 | tf_op jit(solution)/shard_map/all_gather | solution.py:193
  211.6 1.7 copy-start.1
  215.1 1.5 copy-start.2
  216.7 2.1 copy-start.18
  218.8 1.1 copy-start.16
  218.8 2.8 copy-start.15
  218.8 2.8 copy-start.4
  218.8 5.3 %copy-start.14 = (bf16[512,128]{1,0:T(8,128)(2,1)S(1)}, bf16[512,128]{1,0:T(8,128)(2,1)}, u32[]{:S(2)}) copy-start(bf16[512,128]{1,0:T(8,128)(2,1)} %param.32) | copy-start | bytes 393220
  220.9 61.9 %all-gather.13.cloned.1.call-start = ((), (), s32[]{:S(2)}) async-start(), calls=%async_computation.7 | async-start | bytes 1310720 | tf_op jit(solution)/shard_map/all_gather | solution.py:207
  221.5 71.1 %reduce-scatter.5.cloned.1.call-start = ((), (), s32[]{:S(2)}) async-start(), calls=%async_computation.8 | async-start | bytes 983040 | tf_op jit(solution)/shard_map/reduce_scatter | solution.py:209
  221.6 17.9 %collective-permute-start = (bf16[2,512]{1,0:T(2,128)(2,1)S(1)}, bf16[2,512]{1,0:T(2,128)(2,1)S(1)}, u32[]{:S(2)}, u32[]{:S(2)}) collective-permute-start(bf16[2,512]{1,0:T(2,128)(2,1)S(1)} %slice.44), channel_id=1, source_target_pairs={{0,8},{8,16},{16,24},{1,9},{9,17},{17,25},{2,10},{10,18},{18,26},{... | collective-permute-start | bytes 6152 | tf_op jit(solution)/shard_map/ppermute | solution.py:18
Sparse Core Ops, SparseCore 0:
  11.5 42.1 all-gather.6
  55.2 39.4 all-gather.8
  126.6 54.0 reduce-scatter.2
  221.0 30.3 all-gather.10
  252.8 29.8 all-gather.12
  286.2 6.3 reduce-scatter.4
where the time goes:
time: 313 us; the launch traced here: 312 us
  blocking collectives  165 us (53%)
  waiting for transfers between devices  70.9 us (23%)
  local copies, waits for them, and re-layouts  23.9 us (8%)
  matrix products  23.6 us (8%)
  between operations  13.8 us (4%)
  other arithmetic  12 us (4%)
    reduce_scatter x1, waiting for transfers between devices, shards(): lax.psum_scatter(project_in().astype(jnp.bfloat16), 'fs', scatter_dimensi...  36.4 us
    all_gather x1, waiting for transfers between devices, shards(): lax.all_gather(attn_out_weight, 'sp', axis=1, tiled=True)  26.6 us
    all_gather x1, blocking collectives, shards(): lax.all_gather(query_rope_weight, 'sp', axis=0, tiled=True)  22.8 us
    all_gather x1, blocking collectives, shards(): lax.all_gather(latent_weight, 'sp', axis=0, tiled=True)  17.8 us
    all_gather x1, blocking collectives, shards(): latent_piece = lax.all_gather(latent, 'sp', axis=0, tiled=True)  17.8 us
    all_gather x1, blocking collectives, shards(): lax.all_gather(conv_b_weight, 'sp', axis=0, tiled=True)  17.5 us
    all_gather x1, blocking collectives, shards(): lax.all_gather(conv_v_weight, 'sp', axis=0, tiled=True)  16.7 us
    all_gather x1, blocking collectives, shards(): lax.all_gather(conv_c_weight, 'sp', axis=0, tiled=True)  16.5 us
  transfers between devices with their start and end apart: 7, of which 3 were waited for; matrix products, arithmetic and copies ran while one was open for 8% of the time, Pallas kernels for 0%

commit v1 on v0

--- a/solution.py
+++ b/solution.py
@@ -204,7 +204,7 @@
     )
     conv_cols_sp, attn_cols_sp = (
         lax.all_gather(conv_out_weight, "sp", axis=1, tiled=True),
-        lax.all_gather(attn_out_weight, "sp", axis=1, tiled=True),
+        jnp.concatenate(lax.all_gather(attn_out_weight, "sp"), axis=1),
     )
     col_sums = lax.psum_scatter(
         (

time: 313 us -> 293 us (0.936)
  waiting for transfers between devices: 70.9 us -> 43.5 us
  blocking collectives: 165 us -> 171 us
    all_gather x1, waiting for transfers between devices: 26.6 us -> 0.01 us  [shards(): lax.all_gather(attn_out_weight, 'sp')]
    all_gather x1, blocking collectives: 17.8 us -> 24.1 us  [shards(): latent_piece = lax.all_gather(latent, 'sp', axis=0, tiled=True)]
  transfers between devices with their start and end apart: 7 -> 7, of which waited for: 3 -> 2; matrix products, arithmetic and copies ran while one was open for 8% -> 15% of each run, Pallas kernels for 0% -> 0%
where the time goes in v1:
time: 293 us; the launch traced here: 292 us
  blocking collectives  171 us (58%)
  waiting for transfers between devices  43.5 us (15%)
  local copies, waits for them, and re-layouts  24.7 us (8%)
  matrix products  23.3 us (8%)
  between operations  13.8 us (5%)
  other arithmetic  12 us (4%)
  starting transfers between devices  3.08 us (1%)
    reduce_scatter x1, waiting for transfers between devices, shards(): lax.psum_scatter(project_in().astype(jnp.bfloat16), 'fs', scatter_dimensi...  36.4 us
    all_gather x1, blocking collectives, shards(): latent_piece = lax.all_gather(latent, 'sp', axis=0, tiled=True)  24.1 us
    all_gather x1, blocking collectives, shards(): lax.all_gather(query_rope_weight, 'sp', axis=0, tiled=True)  22.8 us
    all_gather x1, blocking collectives, shards(): lax.all_gather(latent_weight, 'sp', axis=0, tiled=True)  17.8 us
    all_gather x1, blocking collectives, shards(): lax.all_gather(conv_b_weight, 'sp', axis=0, tiled=True)  17.5 us
    all_gather x1, blocking collectives, shards(): lax.all_gather(conv_v_weight, 'sp', axis=0, tiled=True)  16.7 us
    all_gather x1, blocking collectives, shards(): lax.all_gather(conv_c_weight, 'sp', axis=0, tiled=True)  16.5 us
    all_gather x1, blocking collectives, shards(): lax.all_gather(conv_out_weight, 'sp', axis=1, tiled=True)  15.8 us
  transfers between devices with their start and end apart: 7, of which 2 were waited for; matrix products, arithmetic and copies ran while one was open for 15% of the time, Pallas kernels for 0%

profile of v1, /device:TPU:0, one launch (start us, length us, event | category | flops | bytes accessed | tf_op | source)
XLA Modules:
  0.0 291.5 jit_solution(10457387778085153424)
XLA Ops:
  6.6 2.7 all-gather
  9.5 1.8 fusion.22
  12.2 17.5 %all_gather.47 = bf16[512,512]{1,0:T(8,128)(2,1)S(1)} all-gather(bf16[128,512]{1,0:T(8,128)(2,1)S(1)} %copy-done.9), channel_id=1, replica_groups=mesh['sp'=4,'fs'=4,'tp'=2] {'sp'}, dimensions={0}, use_global_device_ids=true | all-gather | bytes 655360 | tf_op jit(solution)/shard_map/all_gather | solution.py:78
  29.6 16.5 %all_gather.48 = bf16[512,512]{1,0:T(8,128)(2,1)} all-gather(bf16[128,512]{1,0:T(8,128)(2,1)S(1)} %copy-done.10), channel_id=1, replica_groups=mesh['sp'=4,'fs'=4,'tp'=2] {'sp'}, dimensions={0}, use_global_device_ids=true | all-gather | bytes 655360 | tf_op jit(solution)/shard_map/all_gather | solution.py:79
  46.1 16.7 %all_gather.49 = bf16[512,512]{1,0:T(8,128)(2,1)} all-gather(bf16[128,512]{1,0:T(8,128)(2,1)S(1)} %copy-done.11), channel_id=1, replica_groups=mesh['sp'=4,'fs'=4,'tp'=2] {'sp'}, dimensions={0}, use_global_device_ids=true | all-gather | bytes 655360 | tf_op jit(solution)/shard_map/all_gather | solution.py:80
  62.8 22.8 %all_gather.51 = bf16[512,512]{1,0:T(8,128)(2,1)S(1)} all-gather(bf16[128,512]{1,0:T(8,128)(2,1)S(1)} %copy-done.12), channel_id=1, replica_groups=mesh['sp'=4,'fs'=4,'tp'=2] {'sp'}, dimensions={0}, use_global_device_ids=true | all-gather | bytes 655360 | tf_op jit(solution)/shard_map/all_gather | solution.py:82
  85.6 17.8 %all_gather.52 = bf16[512,512]{1,0:T(8,128)(2,1)} all-gather(bf16[128,512]{1,0:T(8,128)(2,1)S(1)} %copy-done.13), channel_id=1, replica_groups=mesh['sp'=4,'fs'=4,'tp'=2] {'sp'}, dimensions={0}, use_global_device_ids=true | all-gather | bytes 655360 | tf_op jit(solution)/shard_map/all_gather | solution.py:83
  103.4 4.4 %copy.66 = bf16[640,2048]{0,1:T(8,128)(2,1)} copy(bf16[640,2048]{1,0:T(8,128)(2,1)} %all-gather.8.cloned.1.call-done) | data formatting | bytes 5242880 | tf_op jit(solution)/shard_map/all_gather | solution.py:73
  107.8 1.1 constant_dynamic-slice_fusion
  109.9 2.5 convolution_convert_fusion.5
  112.4 1.3 copy.70
  113.8 2.5 convolution_convert_fusion.4
  116.3 1.3 copy.71
  117.6 0.9 constant_dynamic-update-slice_fusion.2
  118.5 0.9 constant_dynamic-update-slice_fusion.1
  119.4 0.9 constant_dynamic-update-slice_fusion
  120.4 3.3 %fusion.15 = bf16[640,3584]{1,0:T(8,128)(2,1)} fusion(bf16[640,3584]{1,0:T(8,128)(2,1)} %constant_dynamic-update-slice_fusion, bf16[640,512]{0,1:T(8,128)(2,1)S(1)} %bitcast.110, bf16[512,1024]{1,0:T(8,128)(2,1)} %all-gather.10.cloned.1.call-done), kind=kOutput, calls=%fused_computation.35 | convolution fusion | flops 671744000 | bytes 3014656 | tf_op jit(solution)/shard_map/dot_general | solution.py:88
  123.6 1.4 fusion.19
  125.0 1.4 fusion.18
  128.4 14.1 %all-gather.2 = bf16[4,160,64]{1,2,0:T(8,128)(2,1)} all-gather(bf16[1,160,64]{1,2,0:T(8,128)(2,1)S(1)} %maximum_bitcast_fusion), channel_id=1, replica_groups=mesh['sp'=4,'fs'=4,'tp'=2] {'sp'}, dimensions={0}, use_global_device_ids=true | all-gather | bytes 102400 | tf_op jit(solution)/shard_map/all_gather | solution.py:161
  142.5 1.9 broadcast_in_dim.56
  144.3 36.4 %reduce-scatter.3.cloned.1.call-done = bf16[160,3584]{1,0:T(8,128)(2,1)} async-done(((bf16[640,3584]{1,0:T(8,128)(2,1)}), bf16[160,3584]{1,0:T(8,128)(2,1)}) %reduce-scatter.3.cloned.1.call-update) | async-done | bytes 1146896 | tf_op jit(solution)/shard_map/reduce_scatter | solution.py:92
  180.7 1.0 fusion.32
  181.8 1.8 fusion.34
  183.6 24.1 %all_gather.55 = bf16[640,512]{1,0:T(8,128)(2,1)S(1)} all-gather(bf16[160,512]{1,0:T(8,128)(2,1)S(1)} %get-tuple-element.251), channel_id=1, replica_groups=mesh['sp'=4,'fs'=4,'tp'=2] {'sp'}, dimensions={0}, use_global_device_ids=true | all-gather | bytes 819200 | tf_op jit(solution)/shard_map/all_gather | solution.py:160
  207.7 0.9 slice_convert_fusion
  209.3 1.5 fusion.16
  210.8 12.1 %conditional.1 = ((f32[160,8]{1,0:T(8,128)S(1)}, f32[160,8,512]{2,1,0:T(8,128)})) conditional(s32[]{:T(128)} %convert_element_type.79, (f32[160,8]{1,0:T(8,128)S(1)}, f32[160,8,512]{2,1,0:T(8,128)}) %tuple.31, (s32[160]{0:T(256)S(1)}, s32[160]{0:T(256)S(1)}, s32[]{:T(128)}, bf16[160,8,512]{2,0,1:T(8,128)(2,1)S(1)}, ...), branch_computations={%region_3.4_spmd, %region_4.7_spmd.clone} | conditional | flops 1792195712 | bytes 46272084 | solution.py:172
  211.1 1.7 copy.87
  212.8 1.7 reshape.213
  214.5 1.5 fusion.9
  215.9 1.9 select_reduce_fusion
  217.9 1.1 fusion.1
  219.6 1.8 multiply_add_fusion
  221.4 1.5 copy-done.2
  222.9 2.1 divide_convert_fusion
  225.1 1.1 multiply_reduce_fusion
  226.2 1.0 copy_bitcast_fusion
  227.3 2.8 collective-permute-start
  230.1 15.8 %all_gather.54 = bf16[512,512]{1,0:T(8,128)(2,1)S(1)} all-gather(bf16[512,128]{1,0:T(8,128)(2,1)S(1)} %copy-done.14), channel_id=1, replica_groups=mesh['sp'=4,'fs'=4,'tp'=2] {'sp'}, dimensions={1}, use_global_device_ids=true | all-gather | bytes 655360 | tf_op jit(solution)/shard_map/all_gather | solution.py:206
  245.9 2.4 copy.83
  248.3 1.0 fusion.40
  249.4 12.0 %all_gather.53 = bf16[640,512]{1,0:T(8,128)(2,1)S(1)} all-gather(bf16[160,512]{1,0:T(8,128)(2,1)S(1)} %fusion.40), channel_id=1, replica_groups=mesh['sp'=4,'fs'=4,'tp'=2] {'fs'}, dimensions={0}, use_global_device_ids=true | all-gather | bytes 819200 | tf_op jit(solution)/shard_map/all_gather | solution.py:192
  262.0 1.5 copy.82
  263.4 3.0 %fusion.17 = bf16[640,512]{1,0:T(8,128)(2,1)} fusion(f32[640,512]{1,0:T(8,128)S(1)} %fusion.44, bf16[640,1024]{1,0:T(8,128)(2,1)S(1)} %bitcast.102, bf16[1024,512]{0,1:T(8,128)(2,1)} %bitcast.106), kind=kOutput, calls=%fused_computation.38 | convolution fusion | flops 671744000 | bytes 4325376 | tf_op jit(solution)/shard_map/dot_general | solution.py:212
  266.4 5.8 %reduce-scatter.5.cloned.1.call-done = bf16[320,512]{1,0:T(8,128)(2,1)} async-done(((bf16[640,512]{1,0:T(8,128)(2,1)}), bf16[320,512]{1,0:T(8,128)(2,1)}) %reduce-scatter.5.cloned.1.call-update) | async-done | bytes 327696 | tf_op jit(solution)/shard_map/reduce_scatter | solution.py:209
  272.2 11.0 %all_to_all.15 = bf16[4,80,512]{2,1,0:T(8,128)(2,1)S(1)} all-to-all(bf16[4,80,512]{2,1,0:T(8,128)(2,1)} %bitcast.113), channel_id=1, replica_groups=mesh['sp'=4,'fs'=4,'tp'=2] {'fs'}, dimensions={0} | all-to-all | bytes 655360 | tf_op jit(solution)/shard_map/all_to_all | solution.py:220
  283.7 1.0 broadcast_in_dim_reshape.4
  (84 shorter events, 6.4 us)
Async XLA Ops:
  6.5 202.8 %copy-start = (bf16[512,1024]{1,0:T(8,128)(2,1)S(1)}, bf16[512,1024]{1,0:T(8,128)(2,1)}, u32[]{:S(2)}) copy-start(bf16[512,1024]{1,0:T(8,128)(2,1)} %param.29) | copy-start | bytes 3145732
  6.5 5.6 %copy-start.9 = (bf16[128,512]{1,0:T(8,128)(2,1)S(1)}, bf16[128,512]{1,0:T(8,128)(2,1)}, u32[]{:S(2)}) copy-start(bf16[128,512]{1,0:T(8,128)(2,1)} %param.20) | copy-start | bytes 393220
  6.5 23.1 %copy-start.10 = (bf16[128,512]{1,0:T(8,128)(2,1)S(1)}, bf16[128,512]{1,0:T(8,128)(2,1)}, u32[]{:S(2)}) copy-start(bf16[128,512]{1,0:T(8,128)(2,1)} %param.21) | copy-start | bytes 393220
  6.5 39.6 %copy-start.11 = (bf16[128,512]{1,0:T(8,128)(2,1)S(1)}, bf16[128,512]{1,0:T(8,128)(2,1)}, u32[]{:S(2)}) copy-start(bf16[128,512]{1,0:T(8,128)(2,1)} %param.22) | copy-start | bytes 393220
  6.5 96.9 %all-gather.8.cloned.1.call-start = ((), (), s32[]{:S(2)}) async-start(), calls=%async_computation.3 | async-start | bytes 3276800 | tf_op jit(solution)/shard_map/all_gather | solution.py:73
  9.3 53.5 %copy-start.12 = (bf16[128,512]{1,0:T(8,128)(2,1)S(1)}, bf16[128,512]{1,0:T(8,128)(2,1)}, u32[]{:S(2)}) copy-start(bf16[128,512]{1,0:T(8,128)(2,1)} %param.25) | copy-start | bytes 393220
  9.3 76.3 %copy-start.13 = (bf16[128,512]{1,0:T(8,128)(2,1)S(1)}, bf16[128,512]{1,0:T(8,128)(2,1)}, u32[]{:S(2)}) copy-start(bf16[128,512]{1,0:T(8,128)(2,1)} %param.26) | copy-start | bytes 393220
  11.4 109.0 %all-gather.10.cloned.1.call-start = ((), (), s32[]{:S(2)}) async-start(), calls=%async_computation.4 | async-start | bytes 1310720 | tf_op jit(solution)/shard_map/all_gather | solution.py:81
  12.1 168.6 %reduce-scatter.3.cloned.1.call-start = ((), (), s32[]{:S(2)}) async-start(), calls=%async_computation.5 | async-start | bytes 5734400 | tf_op jit(solution)/shard_map/reduce_scatter | solution.py:92
  109.0 4.8 %copy-start.5 = (bf16[640,4,1,128]{0,3,2,1:T(8,128)(2,1)}, bf16[640,4,1,128]{0,3,2,1:T(8,128)(2,1)S(1)}, u32[]{:S(2)}) copy-start(bf16[640,4,1,128]{0,3,2,1:T(8,128)(2,1)S(1)} %constant_dynamic-slice_fusion) | copy-start | bytes 1966084
  118.5 1.8 copy-start.6
  120.4 4.7 %copy-start.7 = (bf16[512,512]{1,0:T(8,128)(2,1)S(1)}, bf16[512,512]{1,0:T(8,128)(2,1)}, u32[]{:S(2)}) copy-start(bf16[512,512]{1,0:T(8,128)(2,1)} %all_gather.52) | copy-start | bytes 1572868
  126.5 1.1 copy-start.3
  126.5 1.1 copy-start.8
  126.5 55.3 %copy-start.17 = (f32[512]{0:T(512)S(1)}, f32[512]{0:T(512)}, u32[]{:S(2)}) copy-start(f32[512]{0:T(512)} %param.28) | copy-start | bytes 6148
  126.5 119.4 %all-gather.14.cloned.1.call-start = ((), (), s32[]{:S(2)}) async-start(), calls=%async_computation.8 | async-start | bytes 1310720 | tf_op jit(solution)/shard_map/all_gather | solution.py:207
  127.1 134.9 %all-gather.12.cloned.1.call-start = ((), (), s32[]{:S(2)}) async-start(), calls=%async_computation.6 | async-start | bytes 1638400 | tf_op jit(solution)/shard_map/all_gather | solution.py:193
  217.8 1.7 copy-start.1
  221.4 1.5 copy-start.2
  222.9 2.1 copy-start.18
  225.0 1.1 copy-start.16
  225.1 2.2 copy-start.15
  225.1 2.2 copy-start.4
  225.1 5.1 %copy-start.14 = (bf16[512,128]{1,0:T(8,128)(2,1)S(1)}, bf16[512,128]{1,0:T(8,128)(2,1)}, u32[]{:S(2)}) copy-start(bf16[512,128]{1,0:T(8,128)(2,1)} %param.32) | copy-start | bytes 393220
  227.2 45.0 %reduce-scatter.5.cloned.1.call-start = ((), (), s32[]{:S(2)}) async-start(), calls=%async_computation.7 | async-start | bytes 983040 | tf_op jit(solution)/shard_map/reduce_scatter | solution.py:209
  227.3 21.0 %collective-permute-start = (bf16[2,512]{1,0:T(2,128)(2,1)S(1)}, bf16[2,512]{1,0:T(2,128)(2,1)S(1)}, u32[]{:S(2)}, u32[]{:S(2)}) collective-permute-start(bf16[2,512]{1,0:T(2,128)(2,1)S(1)} %slice.44), channel_id=1, source_target_pairs={{0,8},{8,16},{16,24},{1,9},{9,17},{17,25},{2,10},{10,18},{18,26},{... | collective-permute-start | bytes 6152 | tf_op jit(solution)/shard_map/ppermute | solution.py:18
Sparse Core Ops, SparseCore 0:
  11.5 42.1 all-gather.7
  55.2 39.4 all-gather.9
  126.6 54.0 reduce-scatter.2
  182.2 33.7 all-gather.13
  227.3 31.1 all-gather.11
  266.6 5.6 reduce-scatter.4
